TPU v7x, 256 devices: a whole 4x4x8 slice. The times are simulated.
256 devices in a mesh: kv: 32 (over z, y), tp: 8 (over x, core).
Axes of the slice: x: 4, y: 4, z: 8, core: 2. Of those that a mesh axis runs over, the one named last changes fastest.
Arguments:
- tokens: bfloat16 [64, 4096], P(None, ('kv', 'tp')), may hold values from -8 to 8
- gate_weights: bfloat16 [2, 4096, 11264], P(None, None, ('kv', 'tp')), may hold values from -0.09375 to 0.09375
- up_weights: bfloat16 [2, 4096, 11264], P(None, None, ('kv', 'tp')), may hold values from -0.09375 to 0.09375
- down_weights: bfloat16 [2, 11264, 4096], P(None, ('kv', 'tp')), may hold values from -1 to 1
- norm_gain: bfloat16 [3, 4096], P(None, ('kv', 'tp')), may hold values from 0.25 to 4.5
- norm_bias: bfloat16 [3, 4096], P(None, ('kv', 'tp')), may hold values from -3 to 3
- query_weight: bfloat16 [4096, 4096], P('kv', 'tp'), may hold values from -0.09375 to 0.09375
- forget_weight: bfloat16 [4096, 4096], P('kv', 'tp'), may hold values from -0.09375 to 0.09375
- input_weight: bfloat16 [4096, 4096], P('kv', 'tp'), may hold values from -0.09375 to 0.09375
- outgate_weight: bfloat16 [4096, 4096], P('kv', 'tp'), may hold values from -0.09375 to 0.09375
- lower_bound: float32 [4096], P('tp'), may hold values from 0.05 to 0.9
- head_gain: float32 [4096], P('tp'), may hold values from 0.1 to 1.9
- out_weight: bfloat16 [4096, 4096], P('tp'), may hold values from -0.25 to 0.25
- state: float32 [64, 32, 128, 128], P('kv', 'tp'), may hold values from -3 to 3
Outputs:
- mixed: bfloat16 [64, 4096], P(None, ('kv', 'tp'))
- new_state: float32 [64, 32, 128, 128], P('kv', 'tp')
All inputs are finite; a program needn't handle non-finite values.
Results may differ from a plain program's by a relative error of at most 0.022.
Values may be sent and summed in bfloat16 or wider, within the bound.
A program may use at most 64 MiB of HBM per device.

v0:
```python
import jax
import jax.numpy as jnp
from jax import lax
from jax.sharding import Mesh
from jax.sharding import PartitionSpec as P

HEAD = 128
KV_TP = ("kv_0", "kv_1", "tp_0", "tp_1")
KV = ("kv_0", "kv_1")
TP = ("tp_0", "tp_1")


residual_scale = 8.0**0.25
norm_eps = 1e-05
head_eps = 1e-06


def turned_gather(arrays, axis, dims):
    turned = [jnp.moveaxis(a, dim, 0) for a, dim in zip(arrays, dims)]
    both = jnp.concatenate([t.reshape(len(t), -1) for t in turned], axis=1)
    whole, at, gathered = (lax.all_gather(both, axis, axis=0, tiled=True), 0, [])
    for t, dim in zip(turned, dims):
        section = whole[:, at : at + t[0].size].reshape(-1, *t.shape[1:])
        gathered.append(jnp.moveaxis(section, 0, dim))
        at += t[0].size
    return tuple(gathered)


def rows_for(lines, count):
    spare = -lines.shape[0] % count
    if not spare:
        return lines
    return jnp.concatenate([lines, jnp.zeros((spare, *lines.shape[1:]), lines.dtype)])


def from_everyone(x, axis):
    copies = jnp.broadcast_to(x, (lax.axis_size(axis), *x.shape))
    return lax.all_to_all(copies, axis, split_axis=0, concat_axis=0, tiled=True)


def laid_out(blocks, dim):
    blocks = jnp.moveaxis(blocks, 0, dim)
    shape = blocks.shape
    return blocks.reshape(*shape[:dim], shape[dim] * shape[dim + 1], *shape[dim + 2 :])


def whole_of(x, axes, dim):
    far, near = axes
    leading = from_everyone(x, far)
    blocks = jnp.swapaxes(from_everyone(leading, near), 0, 1)
    return laid_out(blocks.reshape(-1, *x.shape), dim)


def in_blocks(x, dim, count):
    before, after = (x.shape[:dim], x.shape[dim + 1 :])
    return jnp.moveaxis(x.reshape(*before, count, -1, *after), dim, 0)


def sum_at_owner(x, axis, dim):
    blocks = in_blocks(x, dim, lax.axis_size(axis))
    arrived = lax.all_to_all(blocks, axis, split_axis=0, concat_axis=0, tiled=True)
    return arrived.sum(axis=0)


def sum_by_axis(x, axes, dim):
    far, near = axes
    blocks = in_blocks(x, dim, lax.axis_size(far))
    nearer = sum_at_owner(blocks, near, dim + 1)
    arrived = lax.all_to_all(nearer, far, split_axis=0, concat_axis=0, tiled=True)
    return arrived.sum(axis=0)


def nested_sum(x, axes):
    lines = x.reshape(-1)
    padded = rows_for(lines, lax.axis_size(axes[0]) * lax.axis_size(axes[1]))
    whole = whole_of(sum_by_axis(padded, axes, 0), axes, 0)
    return lax.slice_in_dim(whole, 0, len(lines)).reshape(x.shape)


def sum_at_owner_2(x, axis, dim):
    blocks = in_blocks(x, dim, lax.axis_size(axis))
    arrived = lax.all_to_all(blocks, axis, split_axis=0, concat_axis=0, tiled=True)
    return arrived.astype(jnp.float32).sum(axis=0)


def gathered_copies(x, axis, dim):
    blocks = from_everyone(x, axis)
    return laid_out(blocks, dim)


def whole_norm(stream, gain_row, bias_row):
    row_mean = jnp.mean(stream, axis=-1, keepdims=True)
    centred = stream - row_mean
    spread = jnp.mean(centred * centred, axis=-1, keepdims=True)
    return centred * lax.rsqrt(spread + norm_eps) * gain_row.astype(jnp.float32) + bias_row.astype(
        jnp.float32
    )


def ffn_partial(whole_rows, gate_w, up_w, down_w):
    gate_proj = jnp.dot(whole_rows, gate_w, preferred_element_type=jnp.float32)
    up_proj = jnp.dot(whole_rows, up_w, preferred_element_type=jnp.float32)
    hidden = (jax.nn.silu(gate_proj) * up_proj).astype(jnp.bfloat16)
    return jnp.dot(hidden, down_w, preferred_element_type=jnp.float32)


def local(
    tokens,
    gate_weights,
    up_weights,
    down_weights,
    norm_gain,
    norm_bias,
    query_weight,
    forget_weight,
    input_weight,
    outgate_weight,
    lower_bound,
    head_gain,
    out_weight,
    state,
):
    own_cols = tokens.shape[1]
    col_offset = lax.axis_index(KV_TP) * own_cols
    whole_tokens, whole_gain, whole_bias = turned_gather(
        (tokens, norm_gain, norm_bias), KV_TP, (1, 1, 1)
    )

    def finish(partial_value, residual_whole, index, want_whole):
        total = nested_sum(partial_value, (("kv_0", "kv_1"), ("tp_0", "tp_1")))
        stream = residual_scale * residual_whole + 0.5 * total
        normed = whole_norm(stream, whole_gain[index], whole_bias[index]).astype(jnp.bfloat16)
        if want_whole:
            return normed
        return lax.dynamic_slice_in_dim(normed, col_offset, own_cols, 1)

    partial_one = ffn_partial(whole_tokens, gate_weights[0], up_weights[0], down_weights[0])
    normed_one = finish(partial_one, whole_tokens.astype(jnp.float32), 0, True)
    seq_count = state.shape[0]
    head_count = state.shape[1]
    head_cols = query_weight.shape[1]
    weight_rows = query_weight.shape[0]
    seq_offset = lax.axis_index(KV) * seq_count
    block_rows = lax.dynamic_slice_in_dim(
        normed_one, lax.axis_index(KV) * weight_rows, weight_rows, 1
    )
    weights = (query_weight, forget_weight, input_weight, outgate_weight)
    projected = sum_at_owner_2(
        jnp.concatenate(
            [jnp.dot(block_rows, weight, preferred_element_type=jnp.float32) for weight in weights],
            axis=1,
        ).astype(jnp.bfloat16),
        KV,
        0,
    ).astype(jnp.bfloat16)
    query_pre = projected[:, :head_cols].astype(jnp.float32).reshape(seq_count, head_count, HEAD)
    forget_pre = (
        projected[:, head_cols : 2 * head_cols]
        .astype(jnp.float32)
        .reshape(seq_count, head_count, HEAD)
    )
    input_pre = (
        projected[:, 2 * head_cols : 3 * head_cols]
        .astype(jnp.float32)
        .reshape(seq_count, head_count, HEAD)
    )
    outgate_pre = projected[:, 3 * head_cols :].astype(jnp.float32)
    low_bound = lower_bound.reshape(head_count, HEAD)
    forget = low_bound + (1.0 - low_bound) * jax.nn.sigmoid(forget_pre)
    key_part = (1.0 - low_bound) * jax.nn.sigmoid(-forget_pre)
    updated = forget[..., None] * state + key_part[..., None] * input_pre[:, :, None, :]
    readout = jnp.einsum(
        "shd,shde->she", jax.nn.silu(query_pre), updated, precision=lax.Precision.HIGHEST
    )
    readout = readout * lax.rsqrt(jnp.mean(readout * readout, axis=-1, keepdims=True) + head_eps)
    gated_out = (
        readout.reshape(seq_count, head_cols) * head_gain * jax.nn.silu(outgate_pre)
    ).astype(jnp.bfloat16)
    mixer_part = jnp.dot(gated_out, out_weight, preferred_element_type=jnp.float32)
    head_sum = sum_at_owner_2(mixer_part.astype(jnp.bfloat16), TP, 1)
    piece_cols = head_sum.shape[1]
    own_normed = lax.dynamic_slice_in_dim(normed_one, seq_offset, seq_count, 0)
    own_normed = lax.dynamic_slice_in_dim(
        own_normed, lax.axis_index(TP) * piece_cols, piece_cols, 1
    )
    stream_own = (residual_scale * own_normed.astype(jnp.float32) + head_sum).astype(jnp.bfloat16)
    seq_rows = gathered_copies(stream_own, TP, 1)
    stream_two = gathered_copies(seq_rows, KV, 0)
    normed_two = whole_norm(stream_two.astype(jnp.float32), whole_gain[1], whole_bias[1]).astype(
        jnp.bfloat16
    )
    partial_two = ffn_partial(normed_two, gate_weights[1], up_weights[1], down_weights[1])
    mixed = finish(partial_two, normed_two.astype(jnp.float32), 2, False)
    return (mixed, updated)


def solution(mesh):
    finer = Mesh(mesh.devices.reshape(8, 4, 4, 2), ("kv_0", "kv_1", "tp_0", "tp_1"))
    in_specs = (
        P(None, KV_TP),
        P(None, None, KV_TP),
        P(None, None, KV_TP),
        P(None, KV_TP, None),
        P(None, KV_TP),
        P(None, KV_TP),
        P(KV, TP),
        P(KV, TP),
        P(KV, TP),
        P(KV, TP),
        P(TP),
        P(TP),
        P(TP, None),
        P(KV, TP, None, None),
    )
    out_specs = (P(None, KV_TP), P(KV, TP, None, None))
    return jax.shard_map(local, mesh=finer, in_specs=in_specs, out_specs=out_specs, check_vma=False)
```

profile of v0, /device:TPU:1, one launch (start us, length us, event | category | flops | bytes accessed | tf_op | source)
XLA Modules:
  0.0 302.1 jit_solution(11334063490553480618)
XLA Ops:
  3.0 67.7 %all_gather.3 = bf16[4096,70]{1,0:T(8,128)(2,1)S(1)} all-gather(bf16[16,70]{1,0:T(8,128)(2,1)S(1)} %pad_maximum_fusion.1), channel_id=1, replica_groups=mesh['kv_0'=8,'kv_1'=4,'tp_0'=4,'tp_1'=2] {'kv_0','kv_1','tp_0','tp_1'}, dimensions={0}, use_global_device_ids=true | all-gather | bytes 575680 | tf_op jit(solution)/shard_map/all_gather | solution.py:21
  70.8 4.6 %fusion.54 = (bf16[1,44,4096]{2,0,1:T(2,128)(2,1)}, bf16[1,44,4096]{2,0,1:T(2,128)(2,1)}) fusion(bf16[2,44,4096]{2,0,1:T(2,128)(2,1)} %param.17), kind=kLoop, calls=%fused_computation.115 | loop fusion | bytes 1441792 | tf_op jit(solution)/shard_map/slice | solution.py:192
  75.3 2.8 fusion.53
  83.7 18.4 %all_to_all.76 = f32[8,32,1024]{2,1,0:T(8,128)S(1)} all-to-all(f32[8,32,1024]{2,1,0:T(8,128)S(1)} %bitcast.90), channel_id=1, replica_groups=mesh['kv_0'=8,'kv_1'=4,'tp_0'=4,'tp_1'=2] {'tp_0','tp_1'}, dimensions={0} | all-to-all | bytes 2097152 | tf_op jit(solution)/shard_map/all_to_all | solution.py:61
  102.2 14.2 %all_to_all.77 = f32[32,1,1024]{2,1,0:T(1,128)S(1)} all-to-all(f32[32,1,1024]{2,1,0:T(1,128)S(1)} %all_to_all.49), channel_id=1, replica_groups=mesh['kv_0'=8,'kv_1'=4,'tp_0'=4,'tp_1'=2] {'kv_0','kv_1'}, dimensions={0} | all-to-all | bytes 262144 | tf_op jit(solution)/shard_map/all_to_all | solution.py:69
  117.3 3.9 %all-to-all-start.2 = ((f32[32,1,1024]{2,1,0:T(1,128)}), f32[32,1,1024]{2,1,0:T(1,128)S(1)}, u32[]{:S(2)}, u32[]{:S(2)}) async-start(f32[32,1,1024]{2,1,0:T(1,128)} %broadcast_in_dim.12), calls=%async_computation.2 | async-start | bytes 262144 | tf_op jit(solution)/shard_map/all_to_all | solution.py:38
  121.5 9.1 %all-to-all-done.2 = f32[32,1,1024]{2,1,0:T(1,128)S(1)} async-done(((f32[32,1,1024]{2,1,0:T(1,128)}), f32[32,1,1024]{2,1,0:T(1,128)S(1)}, u32[]{:S(2)}, u32[]{:S(2)}) %all-to-all-start.2) | async-done | bytes 131104 | tf_op jit(solution)/shard_map/all_to_all | solution.py:38
  131.7 7.1 %all-to-all-start.3 = ((f32[8,32,1024]{2,1,0:T(8,128)}), f32[8,32,1024]{2,1,0:T(8,128)S(1)}, u32[]{:S(2)}, u32[]{:S(2)}) async-start(f32[8,32,1024]{2,1,0:T(8,128)} %broadcast_in_dim.13), calls=%async_computation.3 | async-start | bytes 2097152 | tf_op jit(solution)/shard_map/all_to_all | solution.py:38
  139.5 3.4 %convert_reduce_fusion = (f32[4096]{0:T(1024)S(1)}, f32[4096]{0:T(1024)S(1)}, f32[4096]{0:T(1024)S(1)}, f32[4096]{0:T(1024)S(1)}, f32[4096]{0:T(1024)S(1)}, /*index=5*/f32[4096]{0:T(1024)S(1)}) fusion(bf16[3,4096]{0,1:T(8,128)(2,1)S(1)} %get-tuple-element.13, bf16[3,4096]{0,1:T(8,128)(2,1)S(1)} %get-tuple-element.12), kind=kLoop, calls=%fused_computation.1 | loop fusion | flops 24576 | bytes 147456 | tf_op jit(solution)/shard_map/add | solution.py:95
  142.8 11.0 %all-to-all-done.3 = f32[8,32,1024]{2,1,0:T(8,128)S(1)} async-done(((f32[8,32,1024]{2,1,0:T(8,128)}), f32[8,32,1024]{2,1,0:T(8,128)S(1)}, u32[]{:S(2)}, u32[]{:S(2)}) %all-to-all-start.3) | async-done | bytes 1048608 | tf_op jit(solution)/shard_map/all_to_all | solution.py:38
  157.7 3.9 %all-to-all-start.4 = ((bf16[32,2,2048]{2,1,0:T(2,128)(2,1)}), bf16[32,2,2048]{2,1,0:T(2,128)(2,1)S(1)}, u32[]{:S(2)}, u32[]{:S(2)}) async-start(bf16[32,2,2048]{2,1,0:T(2,128)(2,1)} %pad_maximum_fusion), calls=%async_computation.4 | async-start | bytes 524288 | tf_op jit(solution)/shard_map/all_to_all | solution.py:82
  161.6 11.4 %all-to-all-done.4 = bf16[32,2,2048]{2,1,0:T(2,128)(2,1)S(1)} async-done(((bf16[32,2,2048]{2,1,0:T(2,128)(2,1)}), bf16[32,2,2048]{2,1,0:T(2,128)(2,1)S(1)}, u32[]{:S(2)}, u32[]{:S(2)}) %all-to-all-start.4) | async-done | bytes 262176 | tf_op jit(solution)/shard_map/all_to_all | solution.py:82
  175.2 3.5 %convolution_convert_fusion = bf16[2,4096]{1,0:T(2,128)(2,1)} fusion(bf16[512,4096]{1,0:T(8,128)(2,1)} %param.26, f32[1,2,4,128]{3,2,1,0:T(4,128)S(1)} %multiply_bitcast_fusion.2, bf16[2,2048]{1,0:T(2,128)(2,1)S(1)} %reduce_sum.124, f32[512]{0:T(512)S(1)} %copy-done.12), kind=kOutput, calls=%fused_computation | convolution fusion | flops 8404992 | bytes 4218880 | tf_op jit(solution)/shard_map/dot_general | solution.py:179
  178.7 5.9 %all-to-all-start.5 = ((bf16[8,2,512]{2,1,0:T(2,128)(2,1)}), bf16[8,2,512]{2,1,0:T(2,128)(2,1)S(1)}, u32[]{:S(2)}, u32[]{:S(2)}) async-start(bf16[8,2,512]{2,1,0:T(2,128)(2,1)} %bitcast.17), calls=%async_computation.5 | async-start | bytes 32768 | tf_op jit(solution)/shard_map/all_to_all | solution.py:82
  184.6 4.7 %all-to-all-done.5 = bf16[8,2,512]{2,1,0:T(2,128)(2,1)S(1)} async-done(((bf16[8,2,512]{2,1,0:T(2,128)(2,1)}), bf16[8,2,512]{2,1,0:T(2,128)(2,1)S(1)}, u32[]{:S(2)}, u32[]{:S(2)}) %all-to-all-start.5) | async-done | bytes 16416 | tf_op jit(solution)/shard_map/all_to_all | solution.py:82
  189.4 7.7 %all_to_all.78 = bf16[8,2,512]{2,1,0:T(2,128)(2,1)S(1)} all-to-all(bf16[8,2,512]{2,1,0:T(2,128)(2,1)S(1)} %broadcast_in_dim.14), channel_id=1, replica_groups=mesh['kv_0'=8,'kv_1'=4,'tp_0'=4,'tp_1'=2] {'tp_0','tp_1'}, dimensions={0} | all-to-all | bytes 32768 | tf_op jit(solution)/shard_map/all_to_all | solution.py:38
  197.6 19.6 %all_to_all.79 = bf16[32,2,4096]{2,1,0:T(2,128)(2,1)S(1)} all-to-all(bf16[32,2,4096]{2,1,0:T(2,128)(2,1)S(1)} %broadcast_in_dim.15), channel_id=1, replica_groups=mesh['kv_0'=8,'kv_1'=4,'tp_0'=4,'tp_1'=2] {'kv_0','kv_1'}, dimensions={0} | all-to-all | bytes 1048576 | tf_op jit(solution)/shard_map/all_to_all | solution.py:38
  220.2 2.2 fusion.3
  223.4 19.7 %all_to_all.80 = f32[8,32,1024]{2,1,0:T(8,128)S(1)} all-to-all(f32[8,32,1024]{2,1,0:T(8,128)S(1)} %bitcast.91), channel_id=1, replica_groups=mesh['kv_0'=8,'kv_1'=4,'tp_0'=4,'tp_1'=2] {'tp_0','tp_1'}, dimensions={0} | all-to-all | bytes 2097152 | tf_op jit(solution)/shard_map/all_to_all | solution.py:61
  243.3 13.5 %all_to_all.81 = f32[32,1,1024]{2,1,0:T(1,128)S(1)} all-to-all(f32[32,1,1024]{2,1,0:T(1,128)S(1)} %all_to_all.59), channel_id=1, replica_groups=mesh['kv_0'=8,'kv_1'=4,'tp_0'=4,'tp_1'=2] {'kv_0','kv_1'}, dimensions={0} | all-to-all | bytes 262144 | tf_op jit(solution)/shard_map/all_to_all | solution.py:69
  257.6 3.9 %all-to-all-start.10 = ((f32[32,1,1024]{2,1,0:T(1,128)}), f32[32,1,1024]{2,1,0:T(1,128)S(1)}, u32[]{:S(2)}, u32[]{:S(2)}) async-start(f32[32,1,1024]{2,1,0:T(1,128)} %broadcast_in_dim.16), calls=%async_computation.10 | async-start | bytes 262144 | tf_op jit(solution)/shard_map/all_to_all | solution.py:38
  262.0 8.9 %all-to-all-done.10 = f32[32,1,1024]{2,1,0:T(1,128)S(1)} async-done(((f32[32,1,1024]{2,1,0:T(1,128)}), f32[32,1,1024]{2,1,0:T(1,128)S(1)}, u32[]{:S(2)}, u32[]{:S(2)}) %all-to-all-start.10) | async-done | bytes 131104 | tf_op jit(solution)/shard_map/all_to_all | solution.py:38
  272.1 7.1 %all-to-all-start.11 = ((f32[8,32,1024]{2,1,0:T(8,128)}), f32[8,32,1024]{2,1,0:T(8,128)S(1)}, u32[]{:S(2)}, u32[]{:S(2)}) async-start(f32[8,32,1024]{2,1,0:T(8,128)} %broadcast_in_dim.17), calls=%async_computation.11 | async-start | bytes 2097152 | tf_op jit(solution)/shard_map/all_to_all | solution.py:38
  280.4 13.8 %all-to-all-done.11 = f32[8,32,1024]{2,1,0:T(8,128)S(1)} async-done(((f32[8,32,1024]{2,1,0:T(8,128)}), f32[8,32,1024]{2,1,0:T(8,128)S(1)}, u32[]{:S(2)}, u32[]{:S(2)}) %all-to-all-start.11) | async-done | bytes 1048608 | tf_op jit(solution)/shard_map/all_to_all | solution.py:38
  (113 shorter events, 33.2 us)
Async XLA Ops:
  0.6 155.3 %copy-start = (bf16[128,512]{1,0:T(8,128)(2,1)S(1)}, bf16[128,512]{1,0:T(8,128)(2,1)}, u32[]{:S(2)}) copy-start(bf16[128,512]{1,0:T(8,128)(2,1)} %param.23) | copy-start | bytes 393220
  0.6 74.7 %copy-start.1 = (bf16[2,4096,44]{1,0,2:T(2,128)(2,1)S(1)}, bf16[2,4096,44]{1,0,2:T(2,128)(2,1)}, u32[]{:S(2)}) copy-start(bf16[2,4096,44]{1,0,2:T(2,128)(2,1)} %param.16) | copy-start | bytes 2162692
  75.3 2.8 copy-start.2
  78.1 2.4 copy-start.6
  117.3 13.3 %all-to-all-start.2 = ((f32[32,1,1024]{2,1,0:T(1,128)}), f32[32,1,1024]{2,1,0:T(1,128)S(1)}, u32[]{:S(2)}, u32[]{:S(2)}) async-start(f32[32,1,1024]{2,1,0:T(1,128)} %broadcast_in_dim.12), calls=%async_computation.2 | async-start | bytes 262144 | tf_op jit(solution)/shard_map/all_to_all | solution.py:38
  131.7 22.1 %all-to-all-start.3 = ((f32[8,32,1024]{2,1,0:T(8,128)}), f32[8,32,1024]{2,1,0:T(8,128)S(1)}, u32[]{:S(2)}, u32[]{:S(2)}) async-start(f32[8,32,1024]{2,1,0:T(8,128)} %broadcast_in_dim.13), calls=%async_computation.3 | async-start | bytes 2097152 | tf_op jit(solution)/shard_map/all_to_all | solution.py:38
  155.3 0.9 copy-start.8
  155.3 1.1 copy-start.9
  155.3 1.3 copy-start.10
  155.6 6.0 %copy-start.11 = (f32[512]{0:T(512)S(1)}, f32[512]{0:T(512)}, u32[]{:S(2)}) copy-start(f32[512]{0:T(512)} %param.24) | copy-start | bytes 6148
  155.6 17.7 %copy-start.7 = (f32[2,4,128,128]{3,2,1,0:T(8,128)S(1)}, f32[2,4,128,128]{3,2,1,0:T(8,128)}, u32[]{:S(2)}) copy-start(f32[2,4,128,128]{3,2,1,0:T(8,128)} %param.27) | copy-start | bytes 1572868
  156.1 19.1 %copy-start.12 = (f32[512]{0:T(512)S(1)}, f32[512]{0:T(512)}, u32[]{:S(2)}) copy-start(f32[512]{0:T(512)} %param.25) | copy-start | bytes 6148
  157.7 15.3 %all-to-all-start.4 = ((bf16[32,2,2048]{2,1,0:T(2,128)(2,1)}), bf16[32,2,2048]{2,1,0:T(2,128)(2,1)S(1)}, u32[]{:S(2)}, u32[]{:S(2)}) async-start(bf16[32,2,2048]{2,1,0:T(2,128)(2,1)} %pad_maximum_fusion), calls=%async_computation.4 | async-start | bytes 524288 | tf_op jit(solution)/shard_map/all_to_all | solution.py:82
  173.7 0.8 copy-start.3
  178.7 10.6 %all-to-all-start.5 = ((bf16[8,2,512]{2,1,0:T(2,128)(2,1)}), bf16[8,2,512]{2,1,0:T(2,128)(2,1)S(1)}, u32[]{:S(2)}, u32[]{:S(2)}) async-start(bf16[8,2,512]{2,1,0:T(2,128)(2,1)} %bitcast.17), calls=%async_computation.5 | async-start | bytes 32768 | tf_op jit(solution)/shard_map/all_to_all | solution.py:82
  197.6 22.1 %copy-start.5 = (bf16[1,4096,44]{1,0,2:T(2,128)(2,1)S(1)}, bf16[1,4096,44]{1,0,2:T(2,128)(2,1)}, u32[]{:S(2)}) copy-start(bf16[1,4096,44]{1,0,2:T(2,128)(2,1)} %get-tuple-element.14) | copy-start | bytes 1081348
  217.2 3.1 %copy-start.4 = (bf16[1,44,4096]{2,0,1:T(2,128)(2,1)S(1)}, bf16[1,44,4096]{2,0,1:T(2,128)(2,1)}, u32[]{:S(2)}) copy-start(bf16[1,44,4096]{2,0,1:T(2,128)(2,1)} %get-tuple-element.18) | copy-start | bytes 1081348
  257.6 13.3 %all-to-all-start.10 = ((f32[32,1,1024]{2,1,0:T(1,128)}), f32[32,1,1024]{2,1,0:T(1,128)S(1)}, u32[]{:S(2)}, u32[]{:S(2)}) async-start(f32[32,1,1024]{2,1,0:T(1,128)} %broadcast_in_dim.16), calls=%async_computation.10 | async-start | bytes 262144 | tf_op jit(solution)/shard_map/all_to_all | solution.py:38
  272.1 22.1 %all-to-all-start.11 = ((f32[8,32,1024]{2,1,0:T(8,128)}), f32[8,32,1024]{2,1,0:T(8,128)S(1)}, u32[]{:S(2)}, u32[]{:S(2)}) async-start(f32[8,32,1024]{2,1,0:T(8,128)} %broadcast_in_dim.17), calls=%async_computation.11 | async-start | bytes 2097152 | tf_op jit(solution)/shard_map/all_to_all | solution.py:38
where the time goes:
time: 303 us; the launch traced here: 302 us
  blocking collectives  161 us (53%)
  waiting for transfers between devices  58.8 us (19%)
  starting transfers between devices  31.7 us (10%)
  local copies, waits for them, and re-layouts  24.7 us (8%)
  other arithmetic  14.9 us (5%)
  matrix products  10 us (3%)
    all_gather x1, blocking collectives, turned_gather(): lax.all_gather(both, axis, axis=0, tiled=True)  67.7 us
    all_to_all x4, waiting for transfers between devices, from_everyone(): return lax.all_to_all(copies, axis, split_axis=0, concat_axis=0, tiled=True)  42.7 us
    all_to_all x2, blocking collectives, sum_at_owner(): lax.all_to_all(blocks, axis, split_axis=0, concat_axis=0, tiled=True)  38.1 us
    all_to_all x2, blocking collectives, sum_by_axis(): lax.all_to_all(nearer, far, split_axis=0, concat_axis=0, tiled=True)  27.8 us
    all_to_all x2, blocking collectives, from_everyone(): return lax.all_to_all(copies, axis, split_axis=0, concat_axis=0, tiled=True)  27.3 us
    all_to_all x4, starting transfers between devices, from_everyone(): return lax.all_to_all(copies, axis, split_axis=0, concat_axis=0, tiled=True)  22 us
    all_to_all x2, waiting for transfers between devices, sum_at_owner_2(): lax.all_to_all(blocks, axis, split_axis=0, concat_axis=0, tiled=True)  16.1 us
    all_to_all x2, starting transfers between devices, sum_at_owner_2(): lax.all_to_all(blocks, axis, split_axis=0, concat_axis=0, tiled=True)  9.75 us
  transfers between devices with their start and end apart: 6, of which 6 were waited for; matrix products, arithmetic and copies ran while one was open for 2% of the time, Pallas kernels for 0%

commit v1 on v0

v1 whole, which is shorter than its diff:
```python
import jax
import jax.numpy as jnp
from jax import lax
from jax.experimental import pallas as pl
from jax.experimental.pallas import tpu as pltpu
from jax.sharding import PartitionSpec as P

MESH = pl.DeviceIdType.MESH
BF = jnp.bfloat16
F32 = jnp.float32
NZ, NY, NX, NC = 8, 4, 4, 2
NT = NX * NC
D = 4096
HEAD = 128
NLT = D // 128
RES = 8.0**0.25
NORM_EPS = 1e-05
HEAD_EPS = 1e-06
ORDER8 = (4, 3, 5, 2, 6, 1, 7)
ORDER4 = (2, 1, 3)
NREMOTE = 256
NLOCAL = 120


def nt_dot(a, b):
    return lax.dot_general(a, b, (((1,), (1,)), ((), ())), preferred_element_type=F32)


def nn_dot(a, b):
    return jnp.dot(a, b, preferred_element_type=F32)


def iota(shape, dim):
    return lax.broadcasted_iota(jnp.int32, shape, dim)


def onehot(mask):
    return jnp.where(mask, 1.0, 0.0).astype(BF)


def f32(v):
    return v.astype(F32)


def kernel(
    tok_h, gate_h, up_h, down_h, gain_h, bias_h, wq_h, wf_h, wi_h, wo_h, lb_h, hg_h, outw_h, state_h,
    mixed_ref, ns_h,
    tok_v, gain_v, bias_v, lb_v, hg_v, gate_r, up_r, down_r, w2g, w2u, d2, w4, outw_v, st_v, ns_v,
    g8, ts, tr, xg, gt, gws, gwr, gws2, gwr2, gwt,
    s0, r0, t0, r1, u0, v0, r2, w0, q0, r3, zb,
    se, st, rz, re, rst, sz, szs, rzs, rze, rzst, rz2,
    sf, rf, yz, yg, xn,
    s1, r0b, t1, r1b, u1, v1, r2b, w1, q1, r3b, sa, ra, sb, rb, sv, rv,
    ssem, rsem, lsem,
):
    kv = lax.axis_index("kv")
    tp = lax.axis_index("tp")
    z, y = lax.div(kv, NY), lax.rem(kv, NY)
    x, c = lax.div(tp, NC), lax.rem(tp, NC)

    def dev(z_=None, y_=None, x_=None, c_=None):
        z_, y_ = z if z_ is None else z_, y if y_ is None else y_
        x_, c_ = x if x_ is None else x_, c if c_ is None else c_
        return (z_ * NY + y_, x_ * NC + c_)

    def zz(d):
        return lax.rem(z + d, NZ)

    def yy(d):
        return lax.rem(y + d, NY)

    def xx(d):
        return lax.rem(x + d, NX)

    oc = 1 - c
    tpeers = [(dx, dc) for dc in (1, 0) for dx in (2, 1, 3, 0) if (dx, dc) != (0, 0)]

    sends = []
    count = [0]

    def slot(n=1):
        first = count[0]
        count[0] += n
        assert count[0] <= NREMOTE
        return first

    def rcopy(i, src, dst, device):
        return pltpu.make_async_remote_copy(
            src_ref=src, dst_ref=dst, send_sem=ssem.at[i], recv_sem=rsem.at[i], device_id=device, device_id_type=MESH
        )

    def send(i, src, dst, device):
        copy = rcopy(i, src, dst, device)
        copy.start()
        sends.append(copy)

    def arrived(i, dst):
        rcopy(i, dst, dst, dev(c_=oc)).wait_recv()

    local = [0]

    def fetch(src, dst):
        i = local[0]
        local[0] += 1
        copy = pltpu.make_async_copy(src, dst, lsem.at[i])
        copy.start()
        return copy

    small = [fetch(tok_h, tok_v), fetch(gain_h, gain_v), fetch(bias_h, bias_v)]

    barrier = pltpu.get_barrier_semaphore()
    peers = [dev(x_=xx(dx), c_=lax.rem(c + dc, NC)) for dx, dc in tpeers]
    peers += [dev(y_=yy(d)) for d in ORDER4] + [dev(z_=zz(d)) for d in ORDER8]
    for p in peers:
        pl.semaphore_signal(barrier, inc=1, device_id=p, device_id_type=MESH)

    def lanes(t):
        return pl.ds(t * 128, 128)

    gate_c = [fetch(gate_h.at[:, :, lanes(t)], gate_r.at[t]) for t in range(NLT)]
    up_c = [fetch(up_h.at[:, :, lanes(t)], up_r.at[t]) for t in range(NLT)]
    down_c = [fetch(down_h.at[:, :, lanes(t)], down_r.at[t]) for t in range(NLT)]
    w4_c = [fetch(w, w4.at[:, pl.ds(512 * i, 512)]) for i, w in enumerate((wq_h, wf_h, wi_h, wo_h))]
    late_c = [fetch(lb_h, lb_v), fetch(hg_h, hg_v), fetch(state_h, st_v), fetch(outw_h, outw_v)]

    for copy in small:
        copy.wait()
    place_t = onehot(iota((128, 16), 0) == tp * 16 + iota((128, 16), 1))
    place = onehot(iota((16, 128), 1) == tp * 16 + iota((16, 128), 0))
    row, col = iota((64, 64), 0), iota((64, 64), 1)
    perm = onehot(col == lax.shift_right_logical(row & 15, 1) * 8 + lax.shift_right_logical(row, 4) * 2 + (row & 1))
    turned = nn_dot(place_t, tok_v[...]).astype(BF)
    token_rows = nt_dot(perm, turned)
    g8[...] = jnp.zeros((8, 128), F32)
    gains = nn_dot(gain_v[...], place)
    biases = nn_dot(bias_v[...], place)
    for i in range(3):
        g8[2 * i : 2 * i + 1, :] = gains[i : i + 1]
        g8[2 * i + 1 : 2 * i + 2, :] = biases[i : i + 1]
    for t in range(NT):
        ts[t] = jnp.concatenate([token_rows[8 * t : 8 * t + 8], g8[...]], axis=0).astype(BF)

    pl.semaphore_wait(barrier, len(peers))

    base = slot(7)
    for i, (dx, dc) in enumerate(tpeers):
        x_, c_ = xx(dx), lax.rem(c + dc, NC)
        send(base + i, ts.at[x_ * NC + c_], tr.at[i], dev(x_=x_, c_=c_))

    def relaid(copies, raw, flat):
        for copy in copies:
            copy.wait()

        def body(t, carry):
            flat[:, pl.ds(pl.multiple_of(t * 128, 128), 128)] = raw[t].reshape(88, 128)
            return carry

        lax.fori_loop(0, NLT, body, 0)

    tile = f32(ts[tp])
    for i in range(7):
        arrived(base + i, tr.at[i])
        tile = tile + f32(tr[i])
    xg[x, c, y, z] = tile[:8].astype(BF)
    gt[y, z] = tile[8:].astype(BF)

    base, gbase = slot(7), slot(7)
    for i, d in enumerate(ORDER8):
        send(base + i, xg.at[x, c, y, z], xg.at[x, c, y, z], dev(z_=zz(d)))
    for i, d in enumerate(ORDER8):
        send(gbase + i, gt.at[y, z], gt.at[y, z], dev(z_=zz(d)))
    relaid(gate_c, gate_r, w2g)
    relaid(up_c, up_r, w2u)
    for i, d in enumerate(ORDER8):
        arrived(base + i, xg.at[x, c, y, zz(NZ - d)])

    ybase, xbase, cbase = slot(3), slot(12), slot(16)
    for i, d in enumerate(ORDER4):
        send(ybase + i, xg.at[x, c, y], xg.at[x, c, y], dev(y_=yy(d)))

    def forward(k, dy):
        yb = yy(NY - dy) if dy else y
        for i, d in enumerate(ORDER4):
            send(xbase + 3 * k + i, xg.at[x, c, yb], xg.at[x, c, yb], dev(x_=xx(d)))
        send(cbase + 4 * k + 3, xg.at[x, c, yb], xg.at[x, c, yb], dev(c_=oc))

    forward(0, 0)
    for i, d in enumerate(ORDER8):
        arrived(gbase + i, gt.at[y, zz(NZ - d)])
    gybase = slot(3)
    for i, d in enumerate(ORDER4):
        send(gybase + i, gt.at[y], gt.at[y], dev(y_=yy(d)))
    for copy in w4_c:
        copy.wait()
    gw = nn_dot(gt[y, z], w4[...])
    gws[...] = gw[:2].astype(BF)
    wbase = slot(3)
    for i, d in enumerate(ORDER4):
        send(wbase + i, gws, gwr.at[i], dev(y_=yy(d)))
    for k, d in enumerate((1, 3, 2)):
        arrived(ybase + ORDER4.index(d), xg.at[x, c, yy(NY - d)])
        forward(k + 1, d)
    relaid(down_c, down_r, d2)
    for k, dy in enumerate((0, 1, 3, 2)):
        yb = yy(NY - dy) if dy else y
        for i, d in enumerate((1, 3, 2)):
            xb = xx(NX - d)
            arrived(xbase + 3 * k + ORDER4.index(d), xg.at[xb, c, yb])
            send(cbase + 4 * k + i, xg.at[xb, c, yb], xg.at[xb, c, yb], dev(c_=oc))
    for k, dy in enumerate((0, 1, 3, 2)):
        yb = yy(NY - dy) if dy else y
        for i, d in enumerate((1, 3, 2)):
            arrived(cbase + 4 * k + i, xg.at[xx(NX - d), oc, yb])
        arrived(cbase + 4 * k + 3, xg.at[x, oc, yb])

    def ffn(whole, which, put):
        gate = nt_dot(whole, w2g[...])
        up = nt_dot(whole, w2u[...])
        hidden = jax.nn.silu(gate) * up
        hidden = jnp.where((iota(hidden.shape, 1) & 1) == which, hidden, 0.0).astype(BF)
        for zb_ in range(NZ):
            part = nn_dot(hidden, d2[:, 512 * zb_ : 512 * zb_ + 512])
            for yb_ in range(NY):
                for t in range(NT):
                    put(t // NC, t % NC, yb_, zb_, part[8 * t : 8 * t + 8, 128 * yb_ : 128 * yb_ + 128].astype(BF))

    def over_core_and_x(s, r, t, rr, u):
        cb, xb_ = slot(4), slot(3)
        for i, d in enumerate((2, 1, 3, 0)):
            x_ = xx(d)
            send(cb + i, s.at[oc, x_], r.at[x_], dev(c_=oc))
        for i, d in enumerate((2, 1, 3)):
            x_ = xx(d)
            arrived(cb + i, r.at[x_])
            t[i] = (f32(s[c, x_]) + f32(r[x_])).astype(BF)
            send(xb_ + i, t.at[i], rr.at[i], dev(x_=x_))
        arrived(cb + 3, r.at[x])
        u[...] = f32(s[c, x]) + f32(r[x])
        for i in range(3):
            arrived(xb_ + i, rr.at[i])
        u[...] = u[...] + f32(rr[0]) + f32(rr[1]) + f32(rr[2])

    whole = jnp.concatenate([xg[:, :, k % NY, k // NY].reshape(64, 128) for k in range(NLT)], axis=1)

    def put0(x_, c_, y_, z_, v):
        s0[c_, x_, y_, z_] = v

    ffn(whole, 0, put0)
    over_core_and_x(s0, r0, t0, r1, u0)
    base = slot(3)
    for i, d in enumerate(ORDER4):
        v0[i] = u0[yy(d)].astype(BF)
        send(base + i, v0.at[i], r2.at[i], dev(y_=yy(d)))
    w0[...] = u0[y]
    for i, d in enumerate(ORDER4):
        arrived(gybase + i, gt.at[yy(NY - d)])
    gw = f32(gws[...])
    for i in range(3):
        arrived(wbase + i, gwr.at[i])
        gw = gw + f32(gwr[i])
    gws2[...] = gw.astype(BF)
    wzbase = slot(7)
    for i, d in enumerate(ORDER8):
        send(wzbase + i, gws2, gwr2.at[i], dev(z_=zz(d)))
    own_tok = f32(xg[x, c])
    shift = RES * jnp.sum(jnp.sum(own_tok, axis=(0, 1)), axis=1, keepdims=True) * (1.0 / D)
    for i in range(3):
        arrived(base + i, r2.at[i])
    w0[...] = w0[...] + f32(r2[0]) + f32(r2[1]) + f32(r2[2])
    base = slot(7)
    for i, d in enumerate(ORDER8):
        q0[i] = w0[zz(d)].astype(BF)
        send(base + i, q0.at[i], r3.at[i], dev(z_=zz(d)))
    total = w0[z]
    for i in range(7):
        arrived(base + i, r3.at[i])
        total = total + f32(r3[i])
    zb[tp] = (RES * f32(xg[x, c, y, z]) + 0.5 * total - shift).astype(BF)
    base = slot(7)
    for i, (dx, dc) in enumerate(tpeers):
        send(base + i, zb.at[tp], zb.at[tp], dev(x_=xx(dx), c_=lax.rem(c + dc, NC)))
    for i, (dx, dc) in enumerate(tpeers):
        from_x, from_c = xx(NX - dx) if dx else x, lax.rem(c + dc, NC)
        arrived(base + i, zb.at[from_x * NC + from_c])

    zv = f32(zb[...].reshape(64, 128))
    mine = f32(gt[y, z])
    proj = nn_dot((zv * mine[0:1]).astype(BF), w4[...])
    for y_ in range(NY):
        se[y_] = proj[16 * y_ : 16 * y_ + 16].astype(BF)
    base = slot(3)
    for i, d in enumerate(ORDER4):
        send(base + i, se.at[yy(d)], re.at[i], dev(y_=yy(d)))
    sums = jnp.where(
        iota((64, 128), 1) < 64,
        jnp.sum(zv, axis=1, keepdims=True),
        jnp.sum(zv * zv, axis=1, keepdims=True),
    )
    for y_ in range(NY):
        st[y_] = sums[16 * y_ : 16 * y_ + 16]
        rzs[y_] = zv[16 * y_ : 16 * y_ + 16].astype(BF)
    sbase, rbase = slot(3), slot(3)
    for i, d in enumerate(ORDER4):
        send(sbase + i, st.at[yy(d)], rst.at[i], dev(y_=yy(d)))
        send(rbase + i, rzs.at[yy(d)], rz.at[y], dev(y_=yy(d)))
    rz[y] = rzs[y]
    gwv = f32(gws2[...])
    for i in range(7):
        arrived(wzbase + i, gwr2.at[i])
        gwv = gwv + f32(gwr2[i])
    gwt[...] = gwv
    for copy in late_c:
        copy.wait()
    acc = f32(se[y])
    for i in range(3):
        arrived(base + i, re.at[i])
        acc = acc + f32(re[i])
    sz[...] = acc.reshape(NZ, 2, 2048).astype(BF)
    base = slot(7)
    for i, d in enumerate(ORDER8):
        send(base + i, sz.at[zz(d)], rze.at[i], dev(z_=zz(d)))
    acc = st[y]
    for i in range(3):
        arrived(sbase + i, rst.at[i])
        acc = acc + rst[i]
    szs[...] = acc.reshape(NZ, 2, 128)
    for i, d in enumerate(ORDER4):
        arrived(rbase + i, rz.at[yy(NY - d)])
    resid = jnp.concatenate([f32(rz[y_]) for y_ in range(NY)], axis=1)
    rz2s = resid.reshape(NZ, 2, 512).astype(BF)
    sv[...] = rz2s
    sbase, rbase = slot(7), slot(7)
    for i, d in enumerate(ORDER8):
        send(sbase + i, szs.at[zz(d)], rzst.at[i], dev(z_=zz(d)))
        send(rbase + i, sv.at[zz(d)], rz2.at[z], dev(z_=zz(d)))
    rz2[z] = sv[z]
    acc = f32(sz[z])
    for i in range(7):
        arrived(base + i, rze.at[i])
        acc = acc + f32(rze[i])
    stat = szs[z]
    for i in range(7):
        arrived(sbase + i, rzst.at[i])
        stat = stat + rzst[i]
    for i, d in enumerate(ORDER8):
        arrived(rbase + i, rz2.at[zz(NZ - d)])
    mean = stat[:, 0:1] * (1.0 / D)
    var = jnp.maximum(stat[:, 64:65] * (1.0 / D) - mean * mean, 0.0)
    scale = lax.rsqrt(var + NORM_EPS)
    proj = (scale * (acc - mean * gwt[0:1]) + gwt[1:2]).astype(BF).astype(F32)

    def by_head(v):
        return jnp.concatenate([v[:, 128 * h : 128 * h + 128] for h in range(4)], axis=0)

    def twice(v):
        return jnp.concatenate([v[h : h + 1] for h in range(4) for _ in range(2)], axis=0)

    query_pre, forget_pre = by_head(proj[:, :512]), by_head(proj[:, 512:1024])
    input_pre, outgate_pre = by_head(proj[:, 1024:1536]), by_head(proj[:, 1536:])
    low, head_gain = twice(lb_v[...]), twice(hg_v[...])
    forget = low + (1.0 - low) * jax.nn.sigmoid(forget_pre)
    key_part = (1.0 - low) * jax.nn.sigmoid(-forget_pre)
    forget_t, key_t, query_t = forget.T, key_part.T, jax.nn.silu(query_pre).T
    reads = []
    for h in range(4):
        for s in range(2):
            i = 2 * h + s
            updated = forget_t[:, i : i + 1] * st_v[s, h] + key_t[:, i : i + 1] * input_pre[i : i + 1]
            ns_v[s, h] = updated
            reads.append(jnp.sum(query_t[:, i : i + 1] * updated, axis=0, keepdims=True))
    ns_copy = fetch(ns_v, ns_h)
    readout = jnp.concatenate(reads, axis=0)
    readout = readout * lax.rsqrt(jnp.mean(readout * readout, axis=1, keepdims=True) + HEAD_EPS)
    gated = readout * head_gain * jax.nn.silu(outgate_pre)
    gated = jnp.concatenate([gated[2 * h : 2 * h + 2] for h in range(4)], axis=1).astype(BF)
    for t in range(NT):
        sf[t] = nn_dot(gated, outw_v[:, 512 * t : 512 * t + 512]).astype(BF)
    base = slot(7)
    for i, (dx, dc) in enumerate(tpeers):
        x_, c_ = xx(dx), lax.rem(c + dc, NC)
        send(base + i, sf.at[x_ * NC + c_], rf.at[i], dev(x_=x_, c_=c_))
    gain_row = jnp.concatenate([f32(gt[y_, tp])[0:1] for y_ in range(NY)], axis=1)
    bias_row = jnp.concatenate([f32(gt[y_, tp])[1:2] for y_ in range(NY)], axis=1)
    normed_one = ((f32(rz2[tp]) - mean) * scale * gain_row + bias_row).astype(BF)
    mix = f32(sf[tp])
    for i in range(7):
        arrived(base + i, rf.at[i])
        mix = mix + f32(rf[i])
    yz[z] = (RES * f32(normed_one) + mix).astype(BF)

    base = slot(7)
    for i, d in enumerate(ORDER8):
        send(base + i, yz.at[z], yz.at[z], dev(z_=zz(d)))
    for i, d in enumerate(ORDER8):
        arrived(base + i, yz.at[zz(NZ - d)])
    yg[x, c, y] = f32(yz[...]).reshape(16, 512).astype(BF)
    ybase, xbase, cbase = slot(3), slot(12), slot(16)
    for i, d in enumerate(ORDER4):
        send(ybase + i, yg.at[x, c, y], yg.at[x, c, y], dev(y_=yy(d)))

    def forward2(k, dy):
        yb = yy(NY - dy) if dy else y
        for i, d in enumerate(ORDER4):
            send(xbase + 3 * k + i, yg.at[x, c, yb], yg.at[x, c, yb], dev(x_=xx(d)))
        send(cbase + 4 * k + 3, yg.at[x, c, yb], yg.at[x, c, yb], dev(c_=oc))

    forward2(0, 0)
    for k, d in enumerate((1, 3, 2)):
        arrived(ybase + ORDER4.index(d), yg.at[x, c, yy(NY - d)])
        forward2(k + 1, d)
    for k, dy in enumerate((0, 1, 3, 2)):
        yb = yy(NY - dy) if dy else y
        for i, d in enumerate((1, 3, 2)):
            xb = xx(NX - d)
            arrived(xbase + 3 * k + ORDER4.index(d), yg.at[xb, c, yb])
            send(cbase + 4 * k + i, yg.at[xb, c, yb], yg.at[xb, c, yb], dev(c_=oc))
    for k, dy in enumerate((0, 1, 3, 2)):
        yb = yy(NY - dy) if dy else y
        for i, d in enumerate((1, 3, 2)):
            arrived(cbase + 4 * k + i, yg.at[xx(NX - d), oc, yb])
        arrived(cbase + 4 * k + 3, yg.at[x, oc, yb])

    streams = [f32(yg[t // NC, t % NC].reshape(64, 512)) for t in range(NT)]
    mean = sum(jnp.sum(v, axis=1, keepdims=True) for v in streams) * (1.0 / D)
    streams = [v - mean for v in streams]
    var = sum(jnp.sum(v * v, axis=1, keepdims=True) for v in streams) * (1.0 / D)
    scale = lax.rsqrt(var + NORM_EPS)
    normed = []
    for t in range(NT):
        gain_row = jnp.concatenate([f32(gt[y_, t])[2:3] for y_ in range(NY)], axis=1)
        bias_row = jnp.concatenate([f32(gt[y_, t])[3:4] for y_ in range(NY)], axis=1)
        normed.append((streams[t] * scale * gain_row + bias_row).astype(BF))
        for y_ in range(NY):
            xn[t, y_] = normed[t][:, 128 * y_ : 128 * y_ + 128].reshape(NT, 8, 128)
    whole = jnp.concatenate(normed, axis=1)

    def put1(x_, c_, y_, z_, v):
        s1[c_, x_, z_, y_] = v

    ffn(whole, 1, put1)
    over_core_and_x(s1, r0b, t1, r1b, u1)
    base = slot(7)
    for i, d in enumerate(ORDER8):
        v1[i] = u1[zz(d)].astype(BF)
        send(base + i, v1.at[i], r2b.at[i], dev(z_=zz(d)))
    w1[...] = u1[z]
    for i in range(7):
        arrived(base + i, r2b.at[i])
        w1[...] = w1[...] + f32(r2b[i])
    q1[...] = w1[...].astype(BF)
    base = slot(3)
    for i, d in enumerate(ORDER4):
        send(base + i, q1, r3b.at[i], dev(y_=yy(d)))
    resid = jnp.concatenate([RES * f32(xn[z, y_, tp]) for y_ in range(NY)], axis=1)
    for i in range(3):
        arrived(base + i, r3b.at[i])
    total = f32(q1[...]) + f32(r3b[0]) + f32(r3b[1]) + f32(r3b[2])
    total = jnp.concatenate([total[y_] for y_ in range(NY)], axis=1)
    stream = resid + 0.5 * total
    for y_ in range(NY):
        w1[y_] = stream[:, 128 * y_ : 128 * y_ + 128]
    rv[tp] = w1[y]
    vbase = slot(7)
    for i, (dx, dc) in enumerate(tpeers):
        send(vbase + i, rv.at[tp], rv.at[tp], dev(x_=xx(dx), c_=lax.rem(c + dc, NC)))

    part_mean = jnp.sum(stream, axis=1, keepdims=True) * (1.0 / 512)
    centred = stream - part_mean
    part_sq = jnp.sum(centred * centred, axis=1, keepdims=True)
    low_half = iota((8, 128), 1) < 64
    sa[...] = jnp.where(low_half, part_mean, part_sq)
    base = slot(7)
    for i, d in enumerate(ORDER8):
        send(base + i, sa, ra.at[i], dev(z_=zz(d)))
    for i in range(7):
        arrived(base + i, ra.at[i])
    parts = [sa[...]] + [ra[i] for i in range(7)]
    means = [p[:, 0:1] for p in parts]
    mean = sum(means) * (1.0 / NZ)
    sq = sum(p[:, 64:65] for p in parts)
    for m in means:
        sq = sq + 512.0 * (m - mean) * (m - mean)
    rb[tp] = jnp.where(low_half, mean, lax.rsqrt(sq * (1.0 / D) + NORM_EPS))
    base = slot(7)
    for i, (dx, dc) in enumerate(tpeers):
        send(base + i, rb.at[tp], rb.at[tp], dev(x_=xx(dx), c_=lax.rem(c + dc, NC)))
    for i, (dx, dc) in enumerate(tpeers):
        source = (xx(NX - dx) if dx else x) * NC + lax.rem(c + dc, NC)
        arrived(vbase + i, rv.at[source])
        arrived(base + i, rb.at[source])
    values, stats = rv[...].reshape(64, 128), rb[...].reshape(64, 128)
    mine = f32(gt[y, z])
    last = ((values - stats[:, 0:1]) * stats[:, 64:65] * mine[4:5] + mine[5:6]).astype(BF)
    picked = nt_dot(place, last).astype(BF)
    mixed_ref[...] = nn_dot(picked, perm).astype(BF)

    ns_copy.wait()
    for copy in sends:
        copy.wait_send()


def vm(*shape, dtype=BF):
    return pltpu.VMEM(shape, dtype)


def local(
    tokens, gate_weights, up_weights, down_weights, norm_gain, norm_bias, query_weight, forget_weight, input_weight,
    outgate_weight, lower_bound, head_gain, out_weight, state,
):
    hbm = pl.BlockSpec(memory_space=pl.ANY)
    f = F32
    scratch = [
        vm(16, 64), vm(3, 16), vm(3, 16), vm(4, 128, dtype=f), vm(4, 128, dtype=f),
        vm(NLT, 44, 2, 128), vm(NLT, 44, 2, 128), vm(NLT, 44, 2, 128), vm(88, D), vm(88, D), vm(88, D),
        vm(128, 2048), vm(512, D), vm(2, 4, 128, 128, dtype=f), vm(2, 4, 128, 128, dtype=f),
        vm(8, 128, dtype=f), vm(NT, 16, 128), vm(7, 16, 128), vm(NX, NC, NY, NZ, 8, 128), vm(NY, NZ, 8, 128),
        vm(2, 2048), vm(3, 2, 2048), vm(2, 2048), vm(7, 2, 2048), vm(2, 2048, dtype=f),
        vm(NC, NX, NY, NZ, 8, 128), vm(NX, NY, NZ, 8, 128), vm(3, NY, NZ, 8, 128), vm(3, NY, NZ, 8, 128),
        vm(NY, NZ, 8, 128, dtype=f), vm(3, NZ, 8, 128), vm(3, NZ, 8, 128), vm(NZ, 8, 128, dtype=f),
        vm(7, 8, 128), vm(7, 8, 128), vm(NT, 8, 128),
        vm(NY, 16, 2048), vm(NY, 16, 128, dtype=f), vm(NY, 16, 128), vm(3, 16, 2048), vm(3, 16, 128, dtype=f),
        vm(NZ, 2, 2048), vm(NZ, 2, 128, dtype=f), vm(NY, 16, 128), vm(7, 2, 2048), vm(7, 2, 128, dtype=f),
        vm(NZ, 2, 512),
        vm(NT, 2, 512), vm(7, 2, 512), vm(NZ, 2, 512), vm(NX, NC, NY, 16, 512), vm(NZ, NY, NT, 8, 128),
        vm(NC, NX, NZ, NY, 8, 128), vm(NX, NZ, NY, 8, 128), vm(3, NZ, NY, 8, 128), vm(3, NZ, NY, 8, 128),
        vm(NZ, NY, 8, 128, dtype=f), vm(7, NY, 8, 128), vm(7, NY, 8, 128), vm(NY, 8, 128, dtype=f),
        vm(NY, 8, 128), vm(3, NY, 8, 128), vm(8, 128, dtype=f), vm(7, 8, 128, dtype=f), vm(1, 8, 128, dtype=f),
        vm(NT, 8, 128, dtype=f), vm(NZ, 2, 512), vm(NT, 8, 128, dtype=f),
        pltpu.SemaphoreType.DMA((NREMOTE,)), pltpu.SemaphoreType.DMA((NREMOTE,)), pltpu.SemaphoreType.DMA((NLOCAL,)),
    ]
    mixed_t, new_state = pl.pallas_call(
        kernel,
        out_shape=(jax.ShapeDtypeStruct((16, 64), BF), jax.ShapeDtypeStruct(state.shape, F32)),
        in_specs=[hbm] * 14,
        out_specs=(pl.BlockSpec(memory_space=pltpu.VMEM), hbm),
        scratch_shapes=scratch,
        compiler_params=pltpu.CompilerParams(
            collective_id=0, has_side_effects=True, vmem_limit_bytes=48 * 1024 * 1024
        ),
        name="decode_step",
    )(
        tokens.T,
        jnp.transpose(gate_weights, (2, 0, 1)),
        jnp.transpose(up_weights, (2, 0, 1)),
        jnp.transpose(down_weights, (1, 0, 2)),
        norm_gain,
        norm_bias,
        query_weight,
        forget_weight,
        input_weight,
        outgate_weight,
        lower_bound.reshape(4, 128),
        head_gain.reshape(4, 128),
        out_weight,
        state,
    )
    return mixed_t.T, new_state


def solution(mesh):
    both = ("kv", "tp")
    in_specs = (
        P(None, both), P(None, None, both), P(None, None, both), P(None, both, None), P(None, both), P(None, both),
        P("kv", "tp"), P("kv", "tp"), P("kv", "tp"), P("kv", "tp"), P("tp"), P("tp"), P("tp", None),
        P("kv", "tp", None, None),
    )
    out_specs = (P(None, both), P("kv", "tp", None, None))
    return jax.shard_map(local, mesh=mesh, in_specs=in_specs, out_specs=out_specs, check_vma=False)
```

time: 303 us -> 117 us (0.39)
  blocking collectives: 161 us -> 0 us
  Pallas kernels: 0 us -> 103 us
  waiting for transfers between devices: 58.8 us -> 0 us
  starting transfers between devices: 31.7 us -> 0 us
  other arithmetic: 14.9 us -> 0 us
  local copies, waits for them, and re-layouts: 24.7 us -> 12.8 us
  matrix products: 10 us -> 0 us
    pallas_call x0 -> x1, Pallas kernels: none -> 103 us  [local(): pl.pallas_call(kernel, out_shape=(jax.ShapeDtypeStruct((16, 64), BF), jax...]
    all_to_all x6 -> x0, blocking collectives: 93.2 us -> none  [the longest x2 38.1 us: sum_at_owner(): lax.all_to_all(blocks, axis, split_axis=0, concat_axis=0, tiled=True)]
    all_gather x1 -> x0, blocking collectives: 67.7 us -> none  [turned_gather(): lax.all_gather(both, axis, axis=0, tiled=True)]
    all_to_all x6 -> x0, waiting for transfers between devices: 58.8 us -> none  [the longest x4 42.7 us: from_everyone(): return lax.all_to_all(copies, axis, split_axis=0, concat_axis=0, tiled=True)]
    all_to_all x6 -> x0, starting transfers between devices: 31.7 us -> none  [the longest x4 22 us: from_everyone(): return lax.all_to_all(copies, axis, split_axis=0, concat_axis=0, tiled=True)]
    dot_general x10 -> x0, matrix products: 10 us -> none  [the longest x2 4.38 us: ffn_partial(): return jnp.dot(hidden, down_w, preferred_element_type=jnp.float32)]
    slice x3 -> x0, local copies, waits for them, and re-layouts: 9.26 us -> none  [the longest x1 4.58 us: local(): down_weights[1]]
    unnamed x34 -> x28, local copies, waits for them, and re-layouts: 3.54 us -> 12.8 us
  transfers between devices with their start and end apart: 6 -> 0, of which waited for: 6 -> 0; matrix products, arithmetic and copies ran while one was open for 2% -> 0% of each run, Pallas kernels for 0% -> 0%
where the time goes in v1:
time: 117 us; the launch traced here: 116 us
  Pallas kernels  103 us (88%)
  local copies, waits for them, and re-layouts  12.8 us (11%)
    pallas_call x1, Pallas kernels, local(): pl.pallas_call(kernel, out_shape=(jax.ShapeDtypeStruct((16, 64), BF), jax...  103 us
    unnamed x28, local copies, waits for them, and re-layouts  12.8 us

profile of v1, /device:TPU:1, one launch (start us, length us, event | category | flops | bytes accessed | tf_op | source)
XLA Modules:
  0.0 116.4 jit_solution(17069194168375951802)
XLA Ops:
  0.6 0.0 copy-start
  0.6 1.1 copy-done
  1.7 0.0 copy-start.1
  1.7 1.1 copy-done.1
  2.9 0.0 copy-start.2
  2.9 1.1 copy-done.2
  4.0 0.0 copy-start.3
  4.0 1.0 copy-done.3
  5.0 0.0 copy-start.4
  5.0 0.9 copy-done.4
  5.9 0.0 copy-start.5
  5.9 0.9 copy-done.5
  6.8 0.0 copy-start.6
  6.8 0.9 copy-done.6
  7.7 0.0 copy-start.7
  7.7 0.9 copy-done.7
  8.6 0.7 copy-done.8
  9.3 0.7 copy-done.9
  10.0 0.7 copy-done.10
  10.7 0.7 copy-done.11
  11.4 0.7 copy-done.12
  12.0 103.0 %decode_step.1 = (bf16[16,64]{1,0:T(8,128)(2,1)S(1)}, f32[2,4,128,128]{3,2,1,0:T(8,128)S(1)}) custom-call(bf16[16,64]{1,0:T(8,128)(2,1)S(1)} %bitcast.10, bf16[44,2,4096]{2,1,0:T(2,128)(2,1)S(1)} %bitcast.7, bf16[44,2,4096]{2,1,0:T(2,128)(2,1)S(1)} %bitcast.8, bf16[44,2,4096]{2,1,0:T(2,128)(2,1)S(1)} %bitcast.9, bf16[3,16]{1,0:T(4,128)(2,1)S(1)} %copy-done.11, ...), custom_call_target="tpu_custom_call" | custom-call | tf_op jit(solution)/shard_map/decode_step/pallas_call | solution.py:531
  115.0 0.6 copy.18
  115.6 0.8 copy.19
  (5 shorter events, 0.0 us)
Async XLA Ops:
  0.6 1.1 copy-start
  1.7 1.1 copy-start.1
  2.9 1.1 copy-start.2
  4.0 1.0 copy-start.3
  5.0 0.9 copy-start.4
  5.9 0.9 copy-start.5
  6.8 0.9 copy-start.6
  7.7 0.9 copy-start.7
  8.6 0.7 copy-start.8
  9.3 0.7 copy-start.9
  10.0 0.7 copy-start.10
  10.7 0.7 copy-start.11
  11.4 0.7 copy-start.12

commit v2 on v1

v2 whole, which is shorter than its diff:
```python
import jax
import jax.numpy as jnp
from jax import lax
from jax.experimental import pallas as pl
from jax.experimental.pallas import tpu as pltpu
from jax.sharding import PartitionSpec as P

MESH = pl.DeviceIdType.MESH
BF = jnp.bfloat16
F32 = jnp.float32
NZ, NY, NX, NC = 8, 4, 4, 2
NT = NX * NC
D = 4096
HEAD = 128
NLT = D // 128
RES = 8.0**0.25
NORM_EPS = 1e-05
HEAD_EPS = 1e-06
ORDER8 = (4, 3, 5, 2, 6, 1, 7)
ORDER4 = (2, 1, 3)
NREMOTE = 80
NLOCAL = 11


def nt_dot(a, b):
    return lax.dot_general(a, b, (((1,), (1,)), ((), ())), preferred_element_type=F32)


def nn_dot(a, b):
    return jnp.dot(a, b, preferred_element_type=F32)


def iota(shape, dim):
    return lax.broadcasted_iota(jnp.int32, shape, dim)


def onehot(mask):
    return jnp.where(mask, 1.0, 0.0).astype(BF)


def f32(v):
    return v.astype(F32)


def kernel(
    tok_h, gate_h, up_h, down_h, gain_h, bias_h, wq_h, wf_h, wi_h, wo_h, lb_h, hg_h, outw_h, state_h,
    mixed_ref, ns_ref,
    tok_v, gain_v, bias_v, lb_v, hg_v, gate_r, up_r, down_r, w2g, w2u, d2, wl, w4, outw_v, st_v,
    g8, ts, tr, xg, gt, gws, gwr, gws2, gwr2, gwt,
    s0, r0, t0, r1, u0, v0, r2, w0, q0, r3, zb, tok_s, shift_s,
    se, st, rz, re, rst, sz, szs, rzs, rze, rzst, rz2,
    sf, rf, yz, yg, xn,
    s1, r0b, t1, r1b, u1, v1, r2b, w1, q1, r3b, sa, ra, rb, sv, rv,
    ssem, rsem, lsem,
):
    kv = lax.axis_index("kv")
    tp = lax.axis_index("tp")
    z, y = lax.div(kv, NY), lax.rem(kv, NY)
    x, c = lax.div(tp, NC), lax.rem(tp, NC)

    oc = 1 - c

    def dev(z_=None, y_=None, x_=None, c_=None):
        z_, y_ = z if z_ is None else z_, y if y_ is None else y_
        x_, c_ = x if x_ is None else x_, c if c_ is None else c_
        return (z_ * NY + y_, x_ * NC + c_)

    def zz(d):
        return lax.rem(z + d, NZ)

    def yy(d):
        return lax.rem(y + d, NY)

    def xx(d):
        return lax.rem(x + d, NX)

    tpeers = [(dx, dc) for dc in (1, 0) for dx in (2, 1, 3, 0) if (dx, dc) != (0, 0)]

    inner, outer = y * oc + x * c, x * oc + y * c

    def step_inner(d):
        return lax.rem(inner + d, 4), dev(y_=lax.rem(y + d * oc, NY), x_=lax.rem(x + d * c, NX))

    def step_outer(d):
        return lax.rem(outer + d, 4), dev(y_=lax.rem(y + d * c, NY), x_=lax.rem(x + d * oc, NX))

    finals = []
    count = [0]

    def slot(n=1):
        first = count[0]
        count[0] += n
        assert count[0] <= NREMOTE
        return first

    def rcopy(i, j, src, dst, device):
        return pltpu.make_async_remote_copy(
            src_ref=src, dst_ref=dst, send_sem=ssem.at[i], recv_sem=rsem.at[j], device_id=device, device_id_type=MESH
        )

    def send(i, j, src, dst, device):
        rcopy(i, j, src, dst, device).start()

    def arrived(j, like):
        rcopy(j, j, like, like, dev(c_=oc)).wait_recv()

    def stage(copies, like):
        i = slot()
        for src, dst, device in copies:
            send(i, i, src, dst, device)
        finals.append((i, like))
        return i

    nlocal = [0]

    def fetch(pairs, like=None):
        i = nlocal[0]
        nlocal[0] += 1
        for src, dst in pairs:
            copy = pltpu.make_async_copy(src, dst, lsem.at[i])
            copy.start()
        return copy if like is None else pltpu.make_async_copy(like, like, lsem.at[i])

    tok_c = fetch([(tok_h, tok_v)])
    gain_c = [fetch([(gain_h, gain_v)]), fetch([(bias_h, bias_v)])]

    barrier = pltpu.get_barrier_semaphore()
    peers = [dev(x_=xx(dx), c_=lax.rem(c + dc, NC)) for dx, dc in tpeers]
    peers += [dev(y_=yy(d)) for d in ORDER4] + [dev(z_=zz(d)) for d in ORDER8]
    for p in peers:
        pl.semaphore_signal(barrier, inc=1, device_id=p, device_id_type=MESH)

    def lanes(t):
        return pl.ds(t * 128, 128)

    gate_c = fetch([(gate_h.at[:, :, lanes(t)], gate_r.at[t]) for t in range(NLT)], gate_r)
    up_c = fetch([(up_h.at[:, :, lanes(t)], up_r.at[t]) for t in range(NLT)], up_r)
    down_c = fetch([(down_h.at[:, :, lanes(t)], down_r.at[t]) for t in range(NLT)], down_r)
    w4_c = fetch([(w, w4.at[:, pl.ds(512 * i, 512)]) for i, w in enumerate((wq_h, wf_h, wi_h, wo_h))], w4)
    late_c = [fetch([(lb_h, lb_v)]), fetch([(hg_h, hg_v)]), fetch([(state_h, st_v)]), fetch([(outw_h, outw_v)])]

    tok_c.wait()
    row, col = iota((128, 64), 0) & 63, iota((128, 64), 1)
    perm2 = onehot(col == lax.shift_right_logical(row & 15, 1) * 8 + lax.shift_right_logical(row, 4) * 2 + (row & 1))
    turned = nt_dot(tok_v[...], perm2)
    xg[c, outer, inner, z] = jnp.where(iota((8, 128), 1) < 64, turned[:8], turned[8:]).astype(BF)
    for copy in gain_c:
        copy.wait()
    place = onehot(iota((16, 128), 1) == tp * 16 + iota((16, 128), 0))
    g8[...] = jnp.zeros((8, 128), F32)
    gains = nn_dot(gain_v[...], place)
    biases = nn_dot(bias_v[...], place)
    for i in range(3):
        g8[2 * i : 2 * i + 1, :] = gains[i : i + 1]
        g8[2 * i + 1 : 2 * i + 2, :] = biases[i : i + 1]
    ts[...] = g8[...].astype(BF)

    lane_in, lane_out = iota((256, 256), 0), iota((256, 256), 1)
    low8, mid, high = lane_in & 7, lax.shift_right_logical(lane_in, 4), lax.shift_right_logical(lane_in, 3) & 1
    shuffle = onehot(lane_out == high * 128 + mid * 8 + low8)
    zeros8 = jnp.zeros((8, 2048), BF)
    for i in range(4):
        wl[96 * i + 88 : 96 * i + 96, :] = zeros8

    def relaid(raw, flat, at):
        for t in range(NLT // 2):
            both = jnp.concatenate([raw[2 * t].reshape(88, 128), raw[2 * t + 1].reshape(88, 128)], axis=1)
            flat[:, 256 * t : 256 * t + 256] = both
            if at is not None:
                moved = nn_dot(both, shuffle).astype(BF)
                wl[at : at + 88, 128 * t : 128 * t + 128] = moved[:, :128]
                wl[at + 96 : at + 184, 128 * t : 128 * t + 128] = moved[:, 128:]

    gate_c.wait()
    relaid(gate_r, w2g, 0)

    pl.semaphore_wait(barrier, len(peers))

    own = xg.at[c, outer, inner, z]
    zs = stage([(own, own, dev(z_=zz(d))) for d in ORDER8], r3)
    gs = stage([(ts, tr.at[i], dev(x_=xx(dx), c_=lax.rem(c + dc, NC))) for i, (dx, dc) in enumerate(tpeers)], r3)
    up_c.wait()
    relaid(up_r, w2u, 192)
    arrived(zs, r3)

    def spread(buf, like3, like16):
        ab, bb, cs = slot(3), slot(4), slot()
        mine = buf.at[c, outer, inner]
        for i, d in enumerate(ORDER4):
            send(ab, ab + i, mine, mine, step_inner(d)[1])
        finals.append((ab, like3))

        def forward(k, at):
            block = buf.at[c, outer, at]
            for d in ORDER4:
                send(bb + k, bb + k, block, block, step_outer(d)[1])
            finals.append((bb + k, like3))
            send(cs, cs, block, block, dev(c_=oc))

        forward(0, inner)
        yield
        order = (1, 3, 2)
        for k, d in enumerate(order):
            at = step_inner(4 - d)[0]
            arrived(ab + ORDER4.index(d), buf.at[c, outer, at])
            forward(k + 1, at)
        yield
        for k, d in enumerate((0, *order)):
            at = step_inner(4 - d)[0] if d else inner
            arrived(bb + k, like3)
            for e in (1, 2, 3):
                block = buf.at[c, step_outer(e)[0], at]
                send(cs, cs, block, block, dev(c_=oc))
        finals.append((cs, like16))
        arrived(cs, like16)
        yield

    gather = spread(xg, r2, r0)
    next(gather)
    arrived(gs, r3)
    tile = f32(ts[...])
    for i in range(7):
        tile = tile + f32(tr[i])
    gt[y, z] = tile.astype(BF)
    own = gt.at[y, z]
    gs = stage([(own, own, dev(z_=zz(d))) for d in ORDER8], r3)
    next(gather)
    w4_c.wait()
    gw = nn_dot(gt[y, z], w4[...])
    gws[...] = gw[:2].astype(BF)
    ws = stage([(gws, gwr.at[i], dev(y_=yy(d))) for i, d in enumerate(ORDER4)], gwr)
    down_c.wait()
    relaid(down_r, d2, None)
    next(gather)

    def down(hidden, put):
        for zb_ in range(NZ):
            part = nn_dot(hidden, d2[:, 512 * zb_ : 512 * zb_ + 512])
            for yb_ in range(NY):
                for t in range(NT):
                    put(t // NC, t % NC, yb_, zb_, part[8 * t : 8 * t + 8, 128 * yb_ : 128 * yb_ + 128].astype(BF))

    def over_core_and(s, r, t, rr, u, me, theirs, step):
        cb, cs, ps = slot(3), slot(), slot()
        at = [(cb, 2), (cb + 1, 1), (cb + 2, 3), (cs, 0)]
        for j, d in at:
            p = lax.rem(theirs + d, 4)
            send(cs, j, s.at[oc, p], r.at[p], dev(c_=oc))
        finals.append((cs, r))
        for i, (j, d) in enumerate(at[:3]):
            p, device = step(d)
            arrived(j, r.at[p])
            t[i] = (f32(s[c, p]) + f32(r[p])).astype(BF)
            send(ps, ps, t.at[i], rr.at[i], device)
        finals.append((ps, rr))
        arrived(cs, r.at[me])
        u[...] = f32(s[c, me]) + f32(r[me])
        arrived(ps, rr)
        u[...] = u[...] + f32(rr[0]) + f32(rr[1]) + f32(rr[2])

    def halves(first):
        return first[0:88, 0:64] + first[96:184, 64:128]

    tiles = [xg[0, x_, y_, z_] if c_ == 0 else xg[1, y_, x_, z_]
             for z_ in range(NZ) for y_ in range(NY) for x_ in range(NX) for c_ in range(NC)]
    whole = jnp.concatenate(tiles, axis=0)
    both = nn_dot(wl[...], whole)
    hidden = jax.nn.silu(halves(both[:192])) * halves(both[192:])
    hidden = jnp.where((iota(hidden.shape, 0) & 1) == 0, hidden, 0.0).T.astype(BF)

    def put0(x_, c_, y_, z_, v):
        if c_ == 0:
            s0[0, x_, y_, z_] = v
        else:
            s0[1, y_, x_, z_] = v

    down(hidden, put0)
    over_core_and(s0, r0, t0, r1, u0, outer, inner, step_outer)
    copies = []
    for i, d in enumerate(ORDER4):
        at, device = step_inner(d)
        v0[i] = u0[at].astype(BF)
        copies.append((v0.at[i], r2.at[i], device))
    rs = stage(copies, r2)
    w0[...] = u0[inner]
    arrived(gs, r3)
    own = gt.at[y]
    gs = stage([(own, own, dev(y_=yy(d))) for d in ORDER4], r2)
    arrived(ws, gwr)
    gw = f32(gws[...])
    for i in range(3):
        gw = gw + f32(gwr[i])
    gws2[...] = gw.astype(BF)
    ws = stage([(gws2, gwr2.at[i], dev(z_=zz(d))) for i, d in enumerate(ORDER8)], gwr2)
    line = jnp.sum(f32(whole).reshape(256, 8, 128), axis=0)
    line = jnp.sum(line, axis=0, keepdims=True) * (RES / D)
    line = line[:, :64] + line[:, 64:]
    shift_s[...] = jnp.broadcast_to(jnp.broadcast_to(line, (8, 64)).T[:, 0:1], (64, 128)).reshape(NT, 8, 128)
    pieces = []
    for m in range(NT):
        piece = f32(xg[0, m // NC, y, z] if m % NC == 0 else xg[1, y, m // NC, z])
        pieces += [piece[:, :64], piece[:, 64:]]
    tok_s[...] = jnp.concatenate(pieces, axis=0).T.reshape(NT, 8, 128)
    base_tile = RES * tok_s[tp] - shift_s[tp]
    arrived(rs, r2)
    w0[...] = w0[...] + f32(r2[0]) + f32(r2[1]) + f32(r2[2])
    copies = []
    for i, d in enumerate(ORDER8):
        q0[i] = w0[zz(d)].astype(BF)
        copies.append((q0.at[i], r3.at[i], dev(z_=zz(d))))
    rs = stage(copies, r3)
    total = w0[z]
    arrived(rs, r3)
    for i in range(7):
        total = total + f32(r3[i])
    zb[tp] = (base_tile + 0.5 * total).astype(BF)
    own = zb.at[tp]
    rs = stage([(own, own, dev(x_=xx(dx), c_=lax.rem(c + dc, NC))) for dx, dc in tpeers], r3)
    arrived(rs, r3)

    def by_head(v):
        return jnp.concatenate([v[:, 128 * h : 128 * h + 128] for h in range(4)], axis=0)

    def twice(v):
        return jnp.concatenate([v[h : h + 1] for h in range(4) for _ in range(2)], axis=0)

    zv = f32(zb[...].reshape(64, 128))
    mine = f32(gt[y, z])
    proj = nn_dot((zv * mine[0:1]).astype(BF), w4[...])
    for y_ in range(NY):
        se[y_] = proj[16 * y_ : 16 * y_ + 16].astype(BF)
    es = stage([(se.at[yy(d)], re.at[i], dev(y_=yy(d))) for i, d in enumerate(ORDER4)], re)
    sums = jnp.where(
        iota((64, 128), 1) < 64,
        jnp.sum(zv, axis=1, keepdims=True),
        jnp.sum(zv * zv, axis=1, keepdims=True),
    )
    for y_ in range(NY):
        st[y_] = sums[16 * y_ : 16 * y_ + 16]
        rzs[y_] = zv[16 * y_ : 16 * y_ + 16].astype(BF)
    fs = stage([(st.at[yy(d)], rst.at[i], dev(y_=yy(d))) for i, d in enumerate(ORDER4)], rst)
    hs = stage([(rzs.at[yy(d)], rz.at[y], dev(y_=yy(d))) for i, d in enumerate(ORDER4)], rz.at[0:3])
    rz[y] = rzs[y]
    arrived(gs, r2)
    arrived(ws, gwr2)
    gwv = f32(gws2[...])
    for i in range(7):
        gwv = gwv + f32(gwr2[i])
    gwt[...] = gwv
    for copy in late_c:
        copy.wait()
    arrived(es, re)
    acc = f32(se[y]) + f32(re[0]) + f32(re[1]) + f32(re[2])
    sz[...] = acc.reshape(NZ, 2, 2048).astype(BF)
    es = stage([(sz.at[zz(d)], rze.at[i], dev(z_=zz(d))) for i, d in enumerate(ORDER8)], rze)
    arrived(fs, rst)
    acc = st[y] + rst[0] + rst[1] + rst[2]
    szs[...] = acc.reshape(NZ, 2, 128)
    fs = stage([(szs.at[zz(d)], rzst.at[i], dev(z_=zz(d))) for i, d in enumerate(ORDER8)], rzst)
    arrived(hs, rz.at[0:3])
    resid = jnp.concatenate([f32(rz[y_]) for y_ in range(NY)], axis=1)
    sv[...] = resid.reshape(NZ, 2, 512).astype(BF)
    hs = stage([(sv.at[zz(d)], rz2.at[z], dev(z_=zz(d))) for i, d in enumerate(ORDER8)], rz2.at[0:7])
    rz2[z] = sv[z]
    low, head_gain = twice(lb_v[...]), twice(hg_v[...])
    gain_row = jnp.concatenate([f32(gt[y_, tp])[0:1] for y_ in range(NY)], axis=1)
    bias_row = jnp.concatenate([f32(gt[y_, tp])[1:2] for y_ in range(NY)], axis=1)
    arrived(fs, rzst)
    stat = szs[z]
    for i in range(7):
        stat = stat + rzst[i]
    mean = stat[:, 0:1] * (1.0 / D)
    var = jnp.maximum(stat[:, 64:65] * (1.0 / D) - mean * mean, 0.0)
    scale = lax.rsqrt(var + NORM_EPS)
    arrived(es, rze)
    acc = f32(sz[z])
    for i in range(7):
        acc = acc + f32(rze[i])
    proj = (scale * (acc - mean * gwt[0:1]) + gwt[1:2]).astype(BF).astype(F32)

    query_pre, forget_pre = by_head(proj[:, :512]), by_head(proj[:, 512:1024])
    input_pre, outgate_pre = by_head(proj[:, 1024:1536]), by_head(proj[:, 1536:])
    forget = low + (1.0 - low) * jax.nn.sigmoid(forget_pre)
    key_part = (1.0 - low) * jax.nn.sigmoid(-forget_pre)
    forget_t, key_t, query_t = forget.T, key_part.T, jax.nn.silu(query_pre).T
    reads = []
    for h in range(4):
        for s in range(2):
            i = 2 * h + s
            updated = forget_t[:, i : i + 1] * st_v[s, h] + key_t[:, i : i + 1] * input_pre[i : i + 1]
            ns_ref[s, h] = updated
            reads.append(jnp.sum(query_t[:, i : i + 1] * updated, axis=0, keepdims=True))
    readout = jnp.concatenate(reads, axis=0)
    readout = readout * lax.rsqrt(jnp.mean(readout * readout, axis=1, keepdims=True) + HEAD_EPS)
    gated = readout * head_gain * jax.nn.silu(outgate_pre)
    gated = jnp.concatenate([gated[2 * h : 2 * h + 2] for h in range(4)], axis=1).astype(BF)
    for t in range(NT):
        sf[t] = nn_dot(gated, outw_v[:, 512 * t : 512 * t + 512]).astype(BF)
    copies = []
    for i, (dx, dc) in enumerate(tpeers):
        x_, c_ = xx(dx), lax.rem(c + dc, NC)
        copies.append((sf.at[x_ * NC + c_], rf.at[i], dev(x_=x_, c_=c_)))
    rs = stage(copies, rf)
    arrived(hs, rz2.at[0:7])
    normed_one = ((f32(rz2[tp]) - mean) * scale * gain_row + bias_row).astype(BF)
    mix = RES * f32(normed_one) + f32(sf[tp])
    arrived(rs, rf)
    for i in range(7):
        mix = mix + f32(rf[i])
    yz[z] = mix.astype(BF)
    own = yz.at[z]
    rs = stage([(own, own, dev(z_=zz(d))) for d in ORDER8], yz.at[0:7])
    arrived(rs, yz.at[0:7])
    yg[c, outer, inner] = f32(yz[...]).reshape(16, 512).astype(BF)
    for _ in spread(yg, yg.at[0, 0, 0:3], yg.at[0]):
        pass

    streams = []
    for t in range(NT):
        blocks = [yg[0, t // NC, y_] if t % NC == 0 else yg[1, y_, t // NC] for y_ in range(NY)]
        streams.append(f32(jnp.concatenate(blocks, axis=0)))
    mean = sum(jnp.sum(v, axis=1, keepdims=True) for v in streams) * (1.0 / D)
    streams = [v - mean for v in streams]
    var = sum(jnp.sum(v * v, axis=1, keepdims=True) for v in streams) * (1.0 / D)
    scale = lax.rsqrt(var + NORM_EPS)
    normed = []
    for t in range(NT):
        gain_row = jnp.concatenate([f32(gt[y_, t])[2:3] for y_ in range(NY)], axis=1)
        bias_row = jnp.concatenate([f32(gt[y_, t])[3:4] for y_ in range(NY)], axis=1)
        normed.append((streams[t] * scale * gain_row + bias_row).astype(BF))
        for y_ in range(NY):
            xn[t, y_] = normed[t][:, 128 * y_ : 128 * y_ + 128].reshape(NT, 8, 128)
    whole = jnp.concatenate(normed, axis=1)

    def put1(x_, c_, y_, z_, v):
        s1[c_, x_, z_, y_] = v

    hidden = jax.nn.silu(nt_dot(whole, w2g[...])) * nt_dot(whole, w2u[...])
    hidden = jnp.where((iota(hidden.shape, 1) & 1) == 1, hidden, 0.0).astype(BF)
    down(hidden, put1)
    over_core_and(s1, r0b, t1, r1b, u1, x, x, lambda d: (xx(d), dev(x_=xx(d))))
    copies = []
    for i, d in enumerate(ORDER8):
        v1[i] = u1[zz(d)].astype(BF)
        copies.append((v1.at[i], r2b.at[i], dev(z_=zz(d))))
    rs = stage(copies, r2b)
    w1[...] = u1[z]
    resid = jnp.concatenate([RES * f32(xn[z, y_, tp]) for y_ in range(NY)], axis=1)
    arrived(rs, r2b)
    acc = w1[...]
    for i in range(7):
        acc = acc + f32(r2b[i])
    q1[...] = acc.astype(BF)
    rs = stage([(q1, r3b.at[i], dev(y_=yy(d))) for i, d in enumerate(ORDER4)], r3b)
    arrived(rs, r3b)
    total = f32(q1[...]) + f32(r3b[0]) + f32(r3b[1]) + f32(r3b[2])
    total = jnp.concatenate([total[y_] for y_ in range(NY)], axis=1)
    stream = resid + 0.5 * total
    part_mean = jnp.sum(stream, axis=1, keepdims=True) * (1.0 / 512)
    centred = stream - part_mean
    part_sq = jnp.sum(centred * centred, axis=1, keepdims=True)
    low_half = iota((8, 128), 1) < 64
    sa[...] = jnp.where(low_half, part_mean, part_sq)
    ss = stage([(sa, ra.at[i], dev(z_=zz(d))) for i, d in enumerate(ORDER8)], ra)
    for y_ in range(NY):
        w1[y_] = stream[:, 128 * y_ : 128 * y_ + 128]
    rv[tp] = w1[y]
    own = rv.at[tp]
    vs = stage([(own, own, dev(x_=xx(dx), c_=lax.rem(c + dc, NC))) for dx, dc in tpeers], rv.at[0:7])
    arrived(ss, ra)
    parts = [sa[...]] + [ra[i] for i in range(7)]
    means = [p[:, 0:1] for p in parts]
    mean = sum(means) * (1.0 / NZ)
    sq = sum(p[:, 64:65] for p in parts)
    for m in means:
        sq = sq + 512.0 * (m - mean) * (m - mean)
    rb[tp] = jnp.where(low_half, mean, lax.rsqrt(sq * (1.0 / D) + NORM_EPS))
    own = rb.at[tp]
    ss = stage([(own, own, dev(x_=xx(dx), c_=lax.rem(c + dc, NC))) for dx, dc in tpeers], rb.at[0:7])
    arrived(vs, rv.at[0:7])
    arrived(ss, rb.at[0:7])
    values, stats = rv[...].reshape(64, 128), rb[...].reshape(64, 128)
    mine = f32(gt[y, z])
    last = ((values - stats[:, 0:1]) * stats[:, 64:65] * mine[4:5] + mine[5:6]).astype(BF)
    picked = nt_dot(place, last).astype(BF)
    mixed_ref[...] = nn_dot(picked, perm2[:64]).astype(BF)

    for i, like in finals:
        rcopy(i, i, like, like, dev(c_=oc)).wait_send()


def vm(*shape, dtype=BF):
    return pltpu.VMEM(shape, dtype)


def local(
    tokens, gate_weights, up_weights, down_weights, norm_gain, norm_bias, query_weight, forget_weight, input_weight,
    outgate_weight, lower_bound, head_gain, out_weight, state,
):
    hbm = pl.BlockSpec(memory_space=pltpu.HBM)
    f = F32
    scratch = [
        vm(16, 64), vm(3, 16), vm(3, 16), vm(4, 128, dtype=f), vm(4, 128, dtype=f),
        vm(NLT, 44, 2, 128), vm(NLT, 44, 2, 128), vm(NLT, 44, 2, 128), vm(88, D), vm(88, D), vm(88, D),
        vm(384, 2048), vm(128, 2048), vm(512, D), vm(2, 4, 128, 128, dtype=f),
        vm(8, 128, dtype=f), vm(8, 128), vm(7, 8, 128), vm(NC, 4, 4, NZ, 8, 128), vm(NY, NZ, 8, 128),
        vm(2, 2048), vm(3, 2, 2048), vm(2, 2048), vm(7, 2, 2048), vm(2, 2048, dtype=f),
        vm(NC, NX, NY, NZ, 8, 128), vm(NX, NY, NZ, 8, 128), vm(3, NY, NZ, 8, 128), vm(3, NY, NZ, 8, 128),
        vm(NY, NZ, 8, 128, dtype=f), vm(3, NZ, 8, 128), vm(3, NZ, 8, 128), vm(NZ, 8, 128, dtype=f),
        vm(7, 8, 128), vm(7, 8, 128), vm(NT, 8, 128), vm(NT, 8, 128, dtype=f), vm(NT, 8, 128, dtype=f),
        vm(NY, 16, 2048), vm(NY, 16, 128, dtype=f), vm(NY, 16, 128), vm(3, 16, 2048), vm(3, 16, 128, dtype=f),
        vm(NZ, 2, 2048), vm(NZ, 2, 128, dtype=f), vm(NY, 16, 128), vm(7, 2, 2048), vm(7, 2, 128, dtype=f),
        vm(NZ, 2, 512),
        vm(NT, 2, 512), vm(7, 2, 512), vm(NZ, 2, 512), vm(NC, 4, 4, 16, 512), vm(NZ, NY, NT, 8, 128),
        vm(NC, NX, NZ, NY, 8, 128), vm(NX, NZ, NY, 8, 128), vm(3, NZ, NY, 8, 128), vm(3, NZ, NY, 8, 128),
        vm(NZ, NY, 8, 128, dtype=f), vm(7, NY, 8, 128), vm(7, NY, 8, 128), vm(NY, 8, 128, dtype=f),
        vm(NY, 8, 128), vm(3, NY, 8, 128), vm(8, 128, dtype=f), vm(7, 8, 128, dtype=f),
        vm(NT, 8, 128, dtype=f), vm(NZ, 2, 512), vm(NT, 8, 128, dtype=f),
        pltpu.SemaphoreType.DMA((NREMOTE,)), pltpu.SemaphoreType.DMA((NREMOTE,)), pltpu.SemaphoreType.DMA((NLOCAL,)),
    ]
    mixed_t, new_state = pl.pallas_call(
        kernel,
        out_shape=(jax.ShapeDtypeStruct((16, 64), BF), jax.ShapeDtypeStruct(state.shape, F32)),
        in_specs=[hbm] * 14,
        out_specs=(pl.BlockSpec(memory_space=pltpu.VMEM), pl.BlockSpec(memory_space=pltpu.VMEM)),
        scratch_shapes=scratch,
        compiler_params=pltpu.CompilerParams(
            collective_id=0, has_side_effects=True, vmem_limit_bytes=40 * 1024 * 1024
        ),
        name="decode_step",
    )(
        tokens.T,
        jnp.transpose(gate_weights, (2, 0, 1)),
        jnp.transpose(up_weights, (2, 0, 1)),
        jnp.transpose(down_weights, (1, 0, 2)),
        norm_gain,
        norm_bias,
        query_weight,
        forget_weight,
        input_weight,
        outgate_weight,
        lower_bound.reshape(4, 128),
        head_gain.reshape(4, 128),
        out_weight,
        state,
    )
    return mixed_t.T, new_state


def solution(mesh):
    both = ("kv", "tp")
    in_specs = (
        P(None, both), P(None, None, both), P(None, None, both), P(None, both, None), P(None, both), P(None, both),
        P("kv", "tp"), P("kv", "tp"), P("kv", "tp"), P("kv", "tp"), P("tp"), P("tp"), P("tp", None),
        P("kv", "tp", None, None),
    )
    out_specs = (P(None, both), P("kv", "tp", None, None))
    return jax.shard_map(local, mesh=mesh, in_specs=in_specs, out_specs=out_specs, check_vma=False)
```

time: 117 us -> 113 us (0.966)
  Pallas kernels: 103 us -> 96.4 us
  local copies, waits for them, and re-layouts: 12.8 us -> 15 us
    pallas_call x1, Pallas kernels: 103 us -> 96.4 us  [local(): pl.pallas_call(kernel, out_shape=(jax.ShapeDtypeStruct((16, 64), BF), jax...]
    unnamed x28 -> x30, local copies, waits for them, and re-layouts: 12.8 us -> 15 us
where the time goes in v2:
time: 113 us; the launch traced here: 112 us
  Pallas kernels  96.4 us (85%)
  local copies, waits for them, and re-layouts  15 us (13%)
    pallas_call x1, Pallas kernels, local(): pl.pallas_call(kernel, out_shape=(jax.ShapeDtypeStruct((16, 64), BF), jax...  96.4 us
    unnamed x30, local copies, waits for them, and re-layouts  15 us

profile of v2, /device:TPU:1, one launch (start us, length us, event | category | flops | bytes accessed | tf_op | source)
XLA Modules:
  0.0 112.0 jit_solution(6650229389391494435)
XLA Ops:
  0.6 0.0 copy-start
  0.6 2.2 %copy-done = bf16[512,4096]{1,0:T(8,128)(2,1)S(1)} copy-done((bf16[512,4096]{1,0:T(8,128)(2,1)S(1)}, bf16[512,4096]{1,0:T(8,128)(2,1)}, u32[]{:S(2)}) %copy-start) | copy-done | bytes 4194328
  2.8 0.0 copy-start.1
  2.8 1.1 copy-done.1
  3.9 0.0 copy-start.2
  3.9 1.1 copy-done.2
  5.0 1.1 copy-done.3
  6.2 0.0 copy-start.4
  6.2 1.0 copy-done.4
  7.2 0.0 copy-start.5
  7.2 0.9 copy-done.5
  8.1 0.0 copy-start.6
  8.1 0.9 copy-done.6
  9.0 0.0 copy-start.7
  9.0 0.9 copy-done.7
  9.9 0.9 copy-done.8
  10.8 0.7 copy-done.9
  11.5 0.7 copy-done.10
  12.2 0.7 copy-done.11
  12.9 0.7 copy-done.12
  13.6 0.7 copy-done.13
  14.2 96.4 %decode_step.1 = (bf16[16,64]{1,0:T(8,128)(2,1)S(1)}, f32[2,4,128,128]{3,2,1,0:T(8,128)S(1)}) custom-call(bf16[16,64]{1,0:T(8,128)(2,1)S(1)} %bitcast.10, bf16[44,2,4096]{2,1,0:T(2,128)(2,1)S(1)} %bitcast.7, bf16[44,2,4096]{2,1,0:T(2,128)(2,1)S(1)} %bitcast.8, bf16[44,2,4096]{2,1,0:T(2,128)(2,1)S(1)} %bitcast.9, bf16[3,16]{1,0:T(4,128)(2,1)S(1)} %copy-done.12, ...), custom_call_target="tpu_custom_call" | custom-call | tf_op jit(solution)/shard_map/decode_step/pallas_call | solution.py:521
  110.6 0.6 copy.18
  111.2 0.8 copy.19
  (7 shorter events, 0.0 us)
Async XLA Ops:
  0.6 2.2 %copy-start = (bf16[512,4096]{1,0:T(8,128)(2,1)S(1)}, bf16[512,4096]{1,0:T(8,128)(2,1)}, u32[]{:S(2)}) copy-start(bf16[512,4096]{1,0:T(8,128)(2,1)} %outw_h.1) | copy-start | bytes 12582916
  2.8 1.1 copy-start.1
  3.9 1.1 copy-start.2
  5.0 1.1 copy-start.3
  6.2 1.0 copy-start.4
  7.2 0.9 copy-start.5
  8.1 0.9 copy-start.6
  9.0 0.9 copy-start.7
  9.9 0.9 copy-start.8
  10.8 0.7 copy-start.9
  11.5 0.7 copy-start.10
  12.2 0.7 copy-start.11
  12.9 0.7 copy-start.12
  13.5 0.7 copy-start.13
